TPU v7x, 32 devices: a whole 2x2x4 slice. The times are simulated.
32 devices in a mesh: grp: 2 (over y), ep: 16 (over z, x, core), tp: 1.
Axes of the slice: x: 2, y: 2, z: 4, core: 2. Of those that a mesh axis runs over, the one named last changes fastest.
Arguments:
- hidden: bfloat16 [256, 2048], P(('grp', 'ep'), 'tp'), parts along dimension 0, may hold values from -6 to 6
- head_input_projected: bfloat16 [256, 2048], P(('grp', 'ep'), 'tp'), parts along dimension 0, may hold values from -6 to 6
- output_gate_projected: bfloat16 [256, 2048], P(('grp', 'ep'), 'tp'), parts along dimension 0, may hold values from -6 to 6
- input_map_projected: bfloat16 [256, 256], P(('grp', 'ep'), 'tp'), parts along dimension 0, may hold values from -0.59765625 to 0.59765625
- output_map_projected: bfloat16 [256, 256], P(('grp', 'ep'), 'tp'), parts along dimension 0, may hold values from -6 to 6
- raw_step_size: bfloat16 [256, 32], P(('grp', 'ep'), 'tp'), parts along dimension 0, may hold values from -5 to 5
- convolution_history: bfloat16 [256, 3, 2048], P(('grp', 'ep'), None, 'tp'), parts along dimension 0, may hold values from -6 to 6
- convolution_kernel: bfloat16 [4, 2048], P(None, 'tp'), may hold values from -3 to 3
- recurrent_state_matrix: float32 [256, 32, 64, 64], P(('grp', 'ep'), 'tp'), parts along dimension 0, may hold values from -0.6 to 0.6
- head_decay_rate: float32 [32], P('tp'), may hold values from 0.05 to 4
- extra_log_decay: float32 [256, 32], P(('grp', 'ep'), 'tp'), parts along dimension 0, may hold values from -0.7 to 0
- head_skip_weight: float32 [32], P('tp'), may hold values from 0.1 to 1.9
- output_matrix: bfloat16 [2048, 2048], P('tp'), may hold values from -0.125 to 0.125
- expert_norm_scale: bfloat16 [2048], replicated, may hold values from 0.099609375 to 1.8984375
- token_expert_index: int32 [256, 6], P(('grp', 'ep')), parts along dimension 0, may hold values from 0 to 15, all different within a row; in each aligned block of 8 rows (0 to 7, 8 to 15, ...) at most 6 rows name the same one
- token_expert_weight: float32 [256, 6], P(('grp', 'ep')), parts along dimension 0, may hold values from 0.2 to 1
- expert_gate_weight: bfloat16 [16, 2048, 704], P('ep', None, 'tp'), may hold values from -0.125 to 0.125
- expert_up_weight: bfloat16 [16, 2048, 704], P('ep', None, 'tp'), may hold values from -0.125 to 0.125
- expert_down_weight: bfloat16 [16, 704, 2048], P('ep', 'tp'), may hold values from -0.21875 to 0.21875
Outputs:
- layer_out: bfloat16 [256, 2048], P(('grp', 'ep'), 'tp'), parts along dimension 0
- new_state: float32 [256, 32, 64, 64], P(('grp', 'ep'), 'tp'), parts along dimension 0
- new_hist: bfloat16 [256, 3, 2048], P(('grp', 'ep'), None, 'tp'), parts along dimension 0
There are 2 independent parts, one for each index of `grp`. A program takes and returns all parts, laid end to end along the dimension named above; an argument that names none is the same for every part. Nothing has to cross between parts.
Inputs may be any that keep to these rules, and one draw needn't show every extreme that they name: `token_expert_index`: in the rows of one device (8 rows), no expert is named more than 6 times, and one expert is named exactly 6 times in some blocks; a token names 6 different experts.
All inputs are finite; a program needn't handle non-finite values.
Results may differ from a plain program's by a relative error of at most 0.015.
Values may be sent and summed in bfloat16 or wider, within the bound.
A program may use at most 64 MiB of HBM per device.

v0:
```python
import functools

import jax
import jax.numpy as jnp
from jax import lax
from jax.experimental import pallas as pl
from jax.experimental.pallas import tpu as pltpu
from jax.sharding import PartitionSpec as P

STATE_DIM = 64
TOPK = 6


EPSILON = 1e-06


def slot_numbers(token_expert_index, capacity, experts):
    flat = token_expert_index.reshape(-1)
    onehot = (flat[:, None] == jnp.arange(experts, dtype=jnp.int32)[None, :]).astype(jnp.int32)
    before = jnp.cumsum(onehot, axis=0) - onehot
    ranks = jnp.sum(before * onehot, axis=1)
    return (flat * capacity + ranks).reshape(token_expert_index.shape)


def on_device(
    hidden,
    head_input_projected,
    output_gate_projected,
    input_map_projected,
    output_map_projected,
    raw_step_size,
    convolution_history,
    convolution_kernel,
    recurrent_state_matrix,
    head_decay_rate,
    extra_log_decay,
    head_skip_weight,
    output_matrix,
    expert_norm_scale,
    token_expert_index,
    token_expert_weight,
    expert_gate_weight,
    expert_up_weight,
    expert_down_weight,
):
    seq_count, inner_local = head_input_projected.shape
    heads_local = raw_step_size.shape[1]
    head_width = inner_local // heads_local
    groups_local = input_map_projected.shape[1] // STATE_DIM
    per_group = heads_local // groups_local
    half_width = hidden.shape[1]
    full_width = output_matrix.shape[1]
    ep_count = lax.axis_size("ep")
    window = jnp.concatenate([convolution_history, head_input_projected[:, None, :]], axis=1)
    new_hist = window[:, 1:]
    conv = jax.nn.silu(
        jnp.sum(window.astype(jnp.float32) * convolution_kernel.astype(jnp.float32)[None], axis=1)
    )
    positive_step_size = jax.nn.softplus(raw_step_size.astype(jnp.float32))
    decay_factor = jnp.exp(-head_decay_rate[None, :] * positive_step_size + extra_log_decay)
    heads_in = conv.reshape(seq_count, heads_local, head_width)
    b_heads = jnp.repeat(
        input_map_projected.astype(jnp.float32).reshape(seq_count, groups_local, STATE_DIM),
        per_group,
        axis=1,
    )
    c_heads = jnp.repeat(
        output_map_projected.astype(jnp.float32).reshape(seq_count, groups_local, STATE_DIM),
        per_group,
        axis=1,
    )
    new_state = (
        decay_factor[:, :, None, None] * recurrent_state_matrix
        + (positive_step_size[:, :, None] * heads_in)[:, :, :, None] * b_heads[:, :, None, :]
    )
    readout = (
        jnp.einsum("shpn,shn->shp", new_state, c_heads) + head_skip_weight[None, :, None] * heads_in
    )
    gated = (
        readout.reshape(seq_count, inner_local)
        * jax.nn.silu(output_gate_projected.astype(jnp.float32))
    ).astype(jnp.bfloat16)
    partial_value = jnp.dot(gated, output_matrix, preferred_element_type=jnp.float32)
    mixed = lax.psum_scatter(
        partial_value.astype(jnp.bfloat16), "tp", scatter_dimension=1, tiled=True
    ).astype(jnp.float32)
    resid = (hidden.astype(jnp.float32) + mixed).astype(jnp.bfloat16)
    capacity = min(seq_count, max(2, 2 * seq_count * TOPK // ep_count))
    total_slots = ep_count * capacity
    slot_ids = jnp.arange(total_slots, dtype=jnp.int32)
    slots = slot_numbers(token_expert_index, capacity, ep_count)
    hits = (slots[:, :, None] == slot_ids[None, None, :]).astype(jnp.float32)
    picks = jnp.sum(hits, axis=1).T.astype(jnp.bfloat16)
    whole_rows = lax.all_gather(resid, "tp", axis=1, tiled=True)
    outgoing = jnp.dot(picks, whole_rows, preferred_element_type=jnp.float32).astype(jnp.bfloat16)
    received = lax.all_to_all(
        outgoing.reshape(ep_count, capacity, full_width),
        "ep",
        split_axis=0,
        concat_axis=0,
        tiled=True,
    )
    expert_rows = received.reshape(total_slots, full_width)
    values = expert_rows.astype(jnp.float32)
    inv_rms = lax.rsqrt(jnp.mean(values * values, axis=1, keepdims=True) + EPSILON)
    scaled = (values * expert_norm_scale.astype(jnp.float32)[None, :]).astype(jnp.bfloat16)
    pre_gate = inv_rms * jnp.dot(scaled, expert_gate_weight[0], preferred_element_type=jnp.float32)
    pre_up = inv_rms * jnp.dot(scaled, expert_up_weight[0], preferred_element_type=jnp.float32)
    act = (jax.nn.silu(pre_gate) * pre_up).astype(jnp.bfloat16)
    down_part = jnp.dot(act, expert_down_weight[0], preferred_element_type=jnp.float32)
    expert_out = lax.psum_scatter(
        down_part.astype(jnp.bfloat16), "tp", scatter_dimension=1, tiled=True
    )
    back = lax.all_to_all(
        expert_out.reshape(ep_count, capacity, half_width),
        "ep",
        split_axis=0,
        concat_axis=0,
        tiled=True,
    )
    mixing = jnp.sum(hits * token_expert_weight[:, :, None], axis=1)
    routed = jnp.dot(
        mixing,
        back.reshape(total_slots, half_width).astype(jnp.float32),
        precision=lax.Precision.HIGHEST,
    )
    layer_out = (resid.astype(jnp.float32) + routed).astype(jnp.bfloat16)
    return (layer_out, new_state, new_hist)


F32, BF16 = jnp.float32, jnp.bfloat16
MESH = pl.DeviceIdType.MESH
LANES = 128
NT = (((1,), (1,)), ((), ()))
VMEM_SPEC = pl.BlockSpec(memory_space=pltpu.VMEM)
HBM_SPEC = pl.BlockSpec(memory_space=pltpu.HBM)
FIELD = LANES // 4
CHUNKS = 4
MIXER_VMEM = 40 * 1024 * 1024
EXPERT_VMEM = 40 * 1024 * 1024


def dot(a, b):
    return jnp.dot(a, b, preferred_element_type=F32)


def three_terms(v):
    hi = v.astype(BF16).astype(F32)
    mid = (v - hi).astype(BF16).astype(F32)
    low = (v - hi - mid).astype(BF16).astype(F32)
    return hi, mid, low


def in_hbm(v):
    return pltpu.with_memory_space_constraint(v, pltpu.HBM)


def sigmoid(v):
    return 1.0 / (1.0 + jnp.exp(-v))


def mixer_kernel(
    hidden_hbm, head_in_hbm, gate_hbm, b_hbm, c_hbm, raw_hbm, hist_hbm, taps_hbm,
    rate_hbm, extra_hbm, skip_hbm, index_hbm, weight_hbm, scale_hbm, state_hbm, wout_hbm,
    packed_ref, resid_ref, state_out, new_hist_out,
    hidden_ref, head_in_ref, gate_ref, b_ref, c_ref, raw_ref, hist_ref, taps_ref,
    rate_ref, extra_ref, skip_ref, index_ref, weight_ref, scale_ref, state_v, wout_v,
    lt, bt, dec, acc, small_sem, in_sem, w_sem, out_sem, hist_sem,
):
    seqs, inner = head_in_ref.shape
    heads = raw_ref.shape[1]
    width = inner // heads
    groups = b_ref.shape[1] // STATE_DIM
    span = inner // groups
    depth = inner // CHUNKS
    full = hidden_ref.shape[1]
    topk = index_ref.shape[1]

    small = [
        pltpu.make_async_copy(a, b, small_sem.at[i])
        for i, (a, b) in enumerate((
            (head_in_hbm, head_in_ref), (hist_hbm, hist_ref), (taps_hbm, taps_ref),
            (raw_hbm, raw_ref), (rate_hbm, rate_ref), (extra_hbm, extra_ref),
            (skip_hbm, skip_ref), (b_hbm, b_ref), (c_hbm, c_ref),
            (gate_hbm, gate_ref), (hidden_hbm, hidden_ref), (index_hbm, index_ref),
            (weight_hbm, weight_ref), (scale_hbm, scale_ref),
        ))
    ]
    for copy in small:
        copy.start()

    def in_copy(s):
        return pltpu.make_async_copy(state_hbm.at[s], state_v.at[s], in_sem.at[s])

    def out_copy(s):
        return pltpu.make_async_copy(state_v.at[s], state_out.at[s], out_sem.at[s])

    def w_copy(k):
        rows = pl.ds(k * depth, depth)
        return pltpu.make_async_copy(wout_hbm.at[rows], wout_v.at[rows], w_sem.at[k])

    for s in range(seqs):
        in_copy(s).start()
    for k in range(CHUNKS):
        w_copy(k).start()

    for copy in small:
        copy.wait()
    hist_copies = (
        pltpu.make_async_copy(hist_ref.at[pl.ds(1, 2)], new_hist_out.at[pl.ds(0, 2)], hist_sem.at[0]),
        pltpu.make_async_copy(head_in_ref, new_hist_out.at[2], hist_sem.at[1]),
    )
    for copy in hist_copies:
        copy.start()
    taps = taps_ref[...].astype(F32)
    head_in = head_in_ref[...]
    total = head_in.astype(F32) * taps[3:4]
    for t in range(3):
        total = total + hist_ref[t].astype(F32) * taps[t:t + 1]
    conv = total * sigmoid(total)

    raw = raw_ref[...].astype(F32)
    step = jnp.maximum(raw, 0.0) + jnp.log(1.0 + jnp.exp(-jnp.abs(raw)))
    dec[...] = jnp.exp(extra_ref[...] - rate_ref[...] * step)
    skip = jnp.broadcast_to(skip_ref[...], (seqs, heads))
    terms = jnp.concatenate(three_terms(step) + three_terms(skip), axis=0).astype(BF16)
    spread = (
        lax.broadcasted_iota(jnp.int32, (heads, inner), 1) // width
        == lax.broadcasted_iota(jnp.int32, (heads, inner), 0)
    ).astype(F32).astype(BF16)
    wide = dot(terms, spread)
    step_wide = wide[0:seqs] + wide[seqs:2 * seqs] + wide[2 * seqs:3 * seqs]
    skip_wide = wide[3 * seqs:4 * seqs] + wide[4 * seqs:5 * seqs] + wide[5 * seqs:6 * seqs]
    pad = jnp.zeros((LANES - 3 * seqs, inner), F32)
    lt[...] = jnp.concatenate(three_terms(step_wide * conv) + (pad,), axis=0).T.astype(BF16)
    b_all = b_ref[...].astype(F32)
    b_pad = jnp.zeros((LANES - 3 * seqs, STATE_DIM), F32)
    for g in range(groups):
        b_g = b_all[:, g * STATE_DIM:(g + 1) * STATE_DIM]
        bt[g] = jnp.concatenate([b_g, b_g, b_g, b_pad], axis=0)
    c_all = c_ref[...].astype(F32)
    c_of = [c_all[:, g * STATE_DIM:(g + 1) * STATE_DIM].astype(BF16) for g in range(groups)]
    k_rows = lax.broadcasted_iota(jnp.int32, (LANES, STATE_DIM), 0)
    s_rows = lax.broadcasted_iota(jnp.int32, (seqs, span), 0)
    acc[...] = jnp.zeros_like(acc)

    def one_sequence(s, carry):
        in_copy(s).wait()
        row = dec[pl.ds(s, 1), :]
        for g in range(groups):
            picked = jnp.where(k_rows % seqs == s, bt[g], 0.0).astype(BF16)
            outer = dot(lt[g * span:(g + 1) * span, :], picked)
            fresh = []
            for j in range(span // width):
                h = g * (span // width) + j
                rows = slice(h * width, (h + 1) * width)
                new = state_v[s, rows, :] * row[:, h:h + 1] + outer[j * width:(j + 1) * width]
                state_v[s, rows, :] = new
                fresh.append(new.astype(BF16))
            read = lax.dot_general(c_of[g], jnp.concatenate(fresh, axis=0), NT, preferred_element_type=F32)
            columns = slice(g * span, (g + 1) * span)
            acc[:, columns] = acc[:, columns] + jnp.where(s_rows == s, read, 0.0)
        out_copy(s).start()
        return carry

    lax.fori_loop(0, seqs, one_sequence, 0)

    gate = gate_ref[...].astype(F32)
    gated = ((acc[...] + skip_wide * conv) * (gate * sigmoid(gate))).astype(BF16)
    mixed = jnp.zeros((seqs, full), F32)
    for k in range(CHUNKS):
        w_copy(k).wait()
        rows = slice(k * depth, (k + 1) * depth)
        mixed = mixed + dot(gated[:, rows], wout_v[rows, :])
    resid = (hidden_ref[...].astype(F32) + mixed.astype(BF16).astype(F32)).astype(BF16)
    resid_ref[...] = resid
    values = resid.astype(F32)
    inv_rms = lax.rsqrt(jnp.mean(values * values, axis=1, keepdims=True) + EPSILON)
    scale = scale_ref[...].reshape(1, full).astype(F32)
    packed_ref[:, :full] = (values * scale).astype(BF16)

    lane = lax.broadcasted_iota(jnp.int32, (seqs, LANES), 1)
    dense = jnp.zeros((seqs, LANES), F32)
    index, weight = index_ref[...], weight_ref[...]
    for k in range(topk):
        dense = dense + jnp.where(lane % FIELD == index[:, k:k + 1], weight[:, k:k + 1], 0.0)
    high = dense.astype(BF16).astype(F32)
    extras = jnp.where(lane < FIELD, high, dense - high)
    for t, term in enumerate(three_terms(inv_rms)):
        extras = jnp.where(lane == 2 * FIELD + t, term, extras)
    packed_ref[:, full:] = extras.astype(BF16)
    for s in range(seqs):
        out_copy(s).wait()
    for copy in hist_copies:
        copy.wait()


def expert_kernel(
    n_ep, packed_ref, resid_ref, wg_hbm, wu_hbm, wd_hbm, out_ref,
    wg, wu, wd, rows_in, act, sent, pair_in, over, over_in, along, along_in,
    w_sem, own_sem, cross_sem, relay_sem, recv_sem, pair_send, pair_recv,
    over_send, over_recv, along_send, along_recv,
):
    me = lax.axis_index("ep")
    line = n_ep // 4
    at, side, core = me // 4, me // 2 % 2, me % 2
    seqs, full = out_ref.shape

    def device(z, x, c):
        return z * 4 + x * 2 + c

    def other(d):
        return (at + d) % line

    partner = device(at, side, 1 - core)
    across = device(at, 1 - side, core)
    barrier = pltpu.get_barrier_semaphore()
    peers = [partner, across] + [device(other(d), side, core) for d in range(1, line)]
    for peer in peers:
        pl.semaphore_signal(barrier, inc=1, device_id={"ep": peer}, device_id_type=MESH)
    weights = [
        pltpu.make_async_copy(a, b, w_sem.at[i])
        for i, (a, b) in enumerate(((wg_hbm, wg), (wu_hbm, wu), (wd_hbm, wd)))
    ]
    for copy in weights:
        copy.start()
    pl.semaphore_wait(barrier, len(peers))

    def remote(src, dst, send, recv, target):
        return pltpu.make_async_remote_copy(
            src_ref=src, dst_ref=dst, send_sem=send, recv_sem=recv,
            device_id={"ep": target}, device_id_type=MESH,
        )

    def slot(z, x, c):
        return (c * 2 + x) * line + z

    def arrived(where):
        remote(packed_ref, rows_in.at[where], own_sem.at[0], recv_sem.at[where], partner).wait_recv()

    started = []

    def start(copy):
        copy.start()
        started.append(copy)

    def forward(where, sem, target):
        start(remote(rows_in.at[where], rows_in.at[where], sem, recv_sem.at[where], target))

    mine = slot(at, side, core)
    for d in range(1, line):
        start(remote(packed_ref, rows_in.at[mine], own_sem.at[d], recv_sem.at[mine], peers[1 + d]))
    start(remote(packed_ref, rows_in.at[mine], own_sem.at[0], recv_sem.at[mine], across))
    start(remote(packed_ref, rows_in.at[mine], own_sem.at[line], recv_sem.at[mine], partner))
    rows_in[mine] = packed_ref[...]

    arrived(slot(at, 1 - side, core))
    forward(slot(at, 1 - side, core), relay_sem.at[0], partner)
    for d in range(line - 1, 0, -1):
        where = slot(other(d), side, core)
        arrived(where)
        forward(where, cross_sem.at[d], across)
        forward(where, relay_sem.at[d], partner)
    for d in range(line - 1, 0, -1):
        where = slot(other(d), 1 - side, core)
        arrived(where)
        forward(where, relay_sem.at[line - 1 + d], partner)
    for x in (side, 1 - side):
        for d in range(line):
            arrived(slot(other(d), x, 1 - core))

    values = rows_in[...].astype(F32).reshape(n_ep * seqs, full + LANES)
    scaled = values[:, :full].astype(BF16)
    extras = values[:, full:]
    lane = lax.broadcasted_iota(jnp.int32, (n_ep * seqs, LANES), 1)

    def total_of(mask):
        return jnp.sum(jnp.where(mask, extras, 0.0), axis=1, keepdims=True)

    share = total_of((lane < 2 * FIELD) & (lane % FIELD == me))
    inv_rms = total_of((lane >= 2 * FIELD) & (lane < 2 * FIELD + 3))
    weights[0].wait()
    pre_gate = inv_rms * lax.dot_general(scaled, wg[...], NT, preferred_element_type=F32)
    weights[1].wait()
    pre_up = inv_rms * lax.dot_general(scaled, wu[...], NT, preferred_element_type=F32)
    act[...] = (pre_gate * sigmoid(pre_gate) * pre_up).astype(BF16)
    weights[2].wait()
    down = dot(act[...], wd[...]).astype(BF16).astype(F32) * share
    sent[...] = down.astype(BF16).reshape(2, 2, line, seqs, full)

    pairs = [
        remote(sent.at[1 - core, x], pair_in.at[x], pair_send.at[i], pair_recv.at[i], partner)
        for i, x in enumerate((1 - side, side))
    ]
    for copy in pairs:
        start(copy)
    pairs[0].wait_recv()
    overs = []
    for d in range(1, line + 1):
        z = other(d)
        over[z] = (sent[core, 1 - side, z].astype(F32) + pair_in[1 - side, z].astype(F32)).astype(BF16)
        overs.append(remote(over.at[z], over_in.at[z], over_send.at[d - 1], over_recv.at[d - 1], across))
        start(overs[-1])
    pairs[1].wait_recv()
    for d in range(1, line):
        z = other(d)
        overs[d - 1].wait_recv()
        here = sent[core, side, z].astype(F32) + pair_in[side, z].astype(F32)
        along[d] = (here + over_in[z].astype(F32)).astype(BF16)
        start(
            remote(along.at[d], along_in.at[d], along_send.at[d], along_recv.at[d], peers[1 + d])
        )
    total = resid_ref[...].astype(F32)
    total = total + sent[core, side, at].astype(F32) + pair_in[side, at].astype(F32)
    overs[line - 1].wait_recv()
    total = total + over_in[at].astype(F32)
    for d in range(1, line):
        remote(along.at[d], along_in.at[d], along_send.at[d], along_recv.at[d], peers[1]).wait_recv()
        total = total + along_in[d].astype(F32)
    out_ref[...] = total.astype(BF16)
    for copy in started:
        copy.wait_send()


def on_device_kernels(
    n_ep,
    hidden,
    head_input_projected,
    output_gate_projected,
    input_map_projected,
    output_map_projected,
    raw_step_size,
    convolution_history,
    convolution_kernel,
    recurrent_state_matrix,
    head_decay_rate,
    extra_log_decay,
    head_skip_weight,
    output_matrix,
    expert_norm_scale,
    token_expert_index,
    token_expert_weight,
    expert_gate_weight,
    expert_up_weight,
    expert_down_weight,
):
    seqs, full = hidden.shape
    inner = head_input_projected.shape[1]
    heads = raw_step_size.shape[1]
    groups = input_map_projected.shape[1] // STATE_DIM
    hidden_units = expert_down_weight.shape[1]
    line = n_ep // 4
    taps = convolution_history.shape[1]
    state = recurrent_state_matrix.reshape(seqs, inner, STATE_DIM)
    dma = pltpu.SemaphoreType.DMA
    operands = (
        hidden, head_input_projected, output_gate_projected, input_map_projected,
        output_map_projected, raw_step_size, jnp.swapaxes(convolution_history, 0, 1),
        convolution_kernel, head_decay_rate.reshape(1, heads), extra_log_decay,
        head_skip_weight.reshape(1, heads), token_expert_index, token_expert_weight,
        expert_norm_scale, state, output_matrix,
    )
    packed, resid, new_state, new_hist = pl.pallas_call(
        mixer_kernel,
        out_shape=(
            pltpu.VMEM((seqs, full + LANES), BF16),
            pltpu.VMEM((seqs, full), BF16),
            pltpu.HBM(state.shape, F32),
            pltpu.HBM((taps, seqs, inner), BF16),
        ),
        in_specs=[HBM_SPEC] * len(operands),
        out_specs=(VMEM_SPEC, VMEM_SPEC, HBM_SPEC, HBM_SPEC),
        scratch_shapes=[pltpu.VMEM(v.shape, v.dtype) for v in operands] + [
            pltpu.VMEM((inner, LANES), BF16),
            pltpu.VMEM((groups, LANES, STATE_DIM), F32),
            pltpu.VMEM((seqs, heads), F32),
            pltpu.VMEM((seqs, inner), F32),
            dma((len(operands) - 2,)),
            dma((seqs,)),
            dma((CHUNKS,)),
            dma((seqs,)),
            dma((2,)),
        ],
        compiler_params=pltpu.CompilerParams(vmem_limit_bytes=MIXER_VMEM),
        name="mixer",
    )(*[in_hbm(v) for v in operands])
    block = (seqs, full)
    layer_out = pl.pallas_call(
        functools.partial(expert_kernel, n_ep),
        out_shape=jax.ShapeDtypeStruct(block, BF16),
        in_specs=[VMEM_SPEC] * 2 + [HBM_SPEC] * 3,
        out_specs=VMEM_SPEC,
        scratch_shapes=[pltpu.VMEM((hidden_units, full), BF16)] * 3 + [
            pltpu.VMEM((n_ep, seqs, full + LANES), BF16),
            pltpu.VMEM((n_ep * seqs, hidden_units), BF16),
            pltpu.VMEM((2, 2, line) + block, BF16),
            pltpu.VMEM((2, line) + block, BF16),
            pltpu.VMEM((line,) + block, BF16),
            pltpu.VMEM((line,) + block, BF16),
            pltpu.VMEM((line,) + block, BF16),
            pltpu.VMEM((line,) + block, BF16),
            dma((3,)),
            dma((line + 1,)),
            dma((line,)),
            dma((2 * line - 1,)),
            dma((n_ep,)),
            dma((2,)),
            dma((2,)),
            dma((line,)),
            dma((line,)),
            dma((line,)),
            dma((line,)),
        ],
        compiler_params=pltpu.CompilerParams(
            collective_id=0, has_side_effects=True, vmem_limit_bytes=EXPERT_VMEM
        ),
        name="experts",
    )(
        packed, resid, in_hbm(jnp.swapaxes(expert_gate_weight[0], 0, 1)),
        in_hbm(jnp.swapaxes(expert_up_weight[0], 0, 1)), in_hbm(expert_down_weight[0]),
    )
    return (
        layer_out, new_state.reshape(recurrent_state_matrix.shape), jnp.swapaxes(new_hist, 0, 1)
    )


def solution(mesh):
    n_ep = mesh.shape["ep"]
    whole_heads = mesh.shape["tp"] == 1 and n_ep % 4 == 0 and 4 < n_ep <= FIELD
    body = functools.partial(on_device_kernels, n_ep) if whole_heads else on_device
    in_specs = (
        P(("grp", "ep"), "tp"),
        P(("grp", "ep"), "tp"),
        P(("grp", "ep"), "tp"),
        P(("grp", "ep"), "tp"),
        P(("grp", "ep"), "tp"),
        P(("grp", "ep"), "tp"),
        P(("grp", "ep"), None, "tp"),
        P(None, "tp"),
        P(("grp", "ep"), "tp", None, None),
        P("tp"),
        P(("grp", "ep"), "tp"),
        P("tp"),
        P("tp", None),
        P(),
        P(("grp", "ep"), None),
        P(("grp", "ep"), None),
        P("ep", None, "tp"),
        P("ep", None, "tp"),
        P("ep", "tp", None),
    )
    out_specs = (
        P(("grp", "ep"), "tp"),
        P(("grp", "ep"), "tp", None, None),
        P(("grp", "ep"), None, "tp"),
    )
    return jax.shard_map(
        body, mesh=mesh, in_specs=in_specs, out_specs=out_specs, check_vma=False
    )
```

profile of v0, /device:TPU:0, one launch (start us, length us, event | category | flops | bytes accessed | tf_op | source)
XLA Modules:
  0.0 38.8 jit_solution(6217039405200688251)
XLA Ops:
  0.6 11.7 %mixer.1 = (bf16[8,2176]{1,0:T(8,128)(2,1)S(1)}, bf16[8,2048]{1,0:T(8,128)(2,1)S(1)}, f32[8,2048,64]{2,1,0:T(8,128)}, bf16[3,8,2048]{2,1,0:T(8,128)(2,1)}) custom-call(bf16[8,2048]{1,0:T(8,128)(2,1)} %hidden_hbm.1, bf16[8,2048]{1,0:T(8,128)(2,1)} %head_in_hbm.1, bf16[8,2048]{1,0:T(8,128)(2,1)} %gate_hbm.1, bf16[8,256]{1,0:T(8,128)(2,1)} %b_hbm.1, ...), custom_call_target="tpu_custom_call" | custom-call | tf_op jit(solution)/shard_map/mixer/pallas_call | solution.py:463
  12.3 25.8 %experts.1 = bf16[8,2048]{1,0:T(8,128)(2,1)S(1)} custom-call(bf16[8,2176]{1,0:T(8,128)(2,1)S(1)} %get-tuple-element.7.packed_ref, bf16[8,2048]{1,0:T(8,128)(2,1)S(1)} %get-tuple-element.8.resid_ref, bf16[704,2048]{1,0:T(8,128)(2,1)} %bitcast.14, bf16[704,2048]{1,0:T(8,128)(2,1)} %bitcast.15, bf16[704,2048]{1,0:T(8,128)(2,1)} %bitcast.16), custom_call_target="tpu_custom_call" | custom-call | tf_op jit(solution)/shard_map/experts/pallas_call | solution.py:488
  38.2 0.6 %copy.23 = bf16[8,2048]{1,0:T(8,128)(2,1)} copy(bf16[8,2048]{1,0:T(8,128)(2,1)S(1)} %experts.1) | data formatting | bytes 65536
where the time goes:
time: 38.9 us; the launch traced here: 38.8 us
  Pallas kernels  37.5 us (96%)
  between operations  0.65 us (2%)
  local copies, waits for them, and re-layouts  0.62 us (2%)
    pallas_call x1, Pallas kernels, on_device_kernels(): pl.pallas_call(functools.partial(expert_kernel, n_ep), out_shape=jax.Shap...  25.8 us
    pallas_call x1, Pallas kernels, on_device_kernels(): pl.pallas_call(mixer_kernel, out_shape=(pltpu.VMEM((seqs, full + LANES),...  11.7 us

commit v1 on v0

--- a/solution.py
+++ b/solution.py
@@ -135,7 +135,6 @@
 VMEM_SPEC = pl.BlockSpec(memory_space=pltpu.VMEM)
 HBM_SPEC = pl.BlockSpec(memory_space=pltpu.HBM)
 FIELD = LANES // 4
-CHUNKS = 4
 MIXER_VMEM = 40 * 1024 * 1024
 EXPERT_VMEM = 40 * 1024 * 1024
 
@@ -165,16 +164,16 @@
     packed_ref, resid_ref, state_out, new_hist_out,
     hidden_ref, head_in_ref, gate_ref, b_ref, c_ref, raw_ref, hist_ref, taps_ref,
     rate_ref, extra_ref, skip_ref, index_ref, weight_ref, scale_ref, state_v, wout_v,
-    lt, bt, dec, acc, small_sem, in_sem, w_sem, out_sem, hist_sem,
+    lt, bt, dec_b, small_sem, in_sem, w_sem, out_sem, hist_sem,
 ):
     seqs, inner = head_in_ref.shape
     heads = raw_ref.shape[1]
     width = inner // heads
     groups = b_ref.shape[1] // STATE_DIM
     span = inner // groups
-    depth = inner // CHUNKS
     full = hidden_ref.shape[1]
     topk = index_ref.shape[1]
+    deep = lt.shape[1]
 
     small = [
         pltpu.make_async_copy(a, b, small_sem.at[i])
@@ -189,20 +188,25 @@
     for copy in small:
         copy.start()
 
-    def in_copy(s):
-        return pltpu.make_async_copy(state_hbm.at[s], state_v.at[s], in_sem.at[s])
-
-    def out_copy(s):
-        return pltpu.make_async_copy(state_v.at[s], state_out.at[s], out_sem.at[s])
-
-    def w_copy(k):
-        rows = pl.ds(k * depth, depth)
-        return pltpu.make_async_copy(wout_hbm.at[rows], wout_v.at[rows], w_sem.at[k])
-
-    for s in range(seqs):
-        in_copy(s).start()
-    for k in range(CHUNKS):
-        w_copy(k).start()
+    def group_rows(g):
+        return pl.ds(g * span, span)
+
+    def in_copy(g):
+        return pltpu.make_async_copy(
+            state_hbm.at[:, group_rows(g)], state_v.at[:, group_rows(g)], in_sem.at[g]
+        )
+
+    def out_copy(g, pair):
+        where = (pl.ds(2 * pair, 2), group_rows(g))
+        return pltpu.make_async_copy(state_v.at[where], state_out.at[where], out_sem.at[g, pair])
+
+    def w_copy(g):
+        return pltpu.make_async_copy(wout_hbm.at[group_rows(g)], wout_v.at[group_rows(g)], w_sem.at[g])
+
+    in_copy(0).start()
+    w_copy(0).start()
+    in_copy(1).start()
+    w_copy(1).start()
 
     for copy in small:
         copy.wait()
@@ -221,57 +225,72 @@
 
     raw = raw_ref[...].astype(F32)
     step = jnp.maximum(raw, 0.0) + jnp.log(1.0 + jnp.exp(-jnp.abs(raw)))
-    dec[...] = jnp.exp(extra_ref[...] - rate_ref[...] * step)
+    decay = jnp.exp(extra_ref[...] - rate_ref[...] * step)
+    for h in range(heads):
+        dec_b[h] = jnp.broadcast_to(decay[:, h:h + 1], (seqs, STATE_DIM))
     skip = jnp.broadcast_to(skip_ref[...], (seqs, heads))
-    terms = jnp.concatenate(three_terms(step) + three_terms(skip), axis=0).astype(BF16)
+    terms = jnp.concatenate(three_terms(step) + three_terms(skip) + three_terms(decay), axis=0).astype(BF16)
     spread = (
         lax.broadcasted_iota(jnp.int32, (heads, inner), 1) // width
         == lax.broadcasted_iota(jnp.int32, (heads, inner), 0)
     ).astype(F32).astype(BF16)
     wide = dot(terms, spread)
-    step_wide = wide[0:seqs] + wide[seqs:2 * seqs] + wide[2 * seqs:3 * seqs]
-    skip_wide = wide[3 * seqs:4 * seqs] + wide[4 * seqs:5 * seqs] + wide[5 * seqs:6 * seqs]
-    pad = jnp.zeros((LANES - 3 * seqs, inner), F32)
-    lt[...] = jnp.concatenate(three_terms(step_wide * conv) + (pad,), axis=0).T.astype(BF16)
+
+    def widened(i):
+        at = 3 * i * seqs
+        return wide[at:at + seqs] + wide[at + seqs:at + 2 * seqs] + wide[at + 2 * seqs:at + 3 * seqs]
+
+    step_wide, skip_wide, decay_wide = widened(0), widened(1), widened(2)
+    fed = step_wide * conv
+    pad = jnp.zeros((deep - 3 * seqs, inner), F32)
+    lt[...] = jnp.concatenate(three_terms(fed) + (pad,), axis=0).T.astype(BF16)
     b_all = b_ref[...].astype(F32)
-    b_pad = jnp.zeros((LANES - 3 * seqs, STATE_DIM), F32)
+    c_all = c_ref[...].astype(F32)
+    b_rows = lax.broadcasted_iota(jnp.int32, (deep, LANES), 0)
+    c_rows = lax.broadcasted_iota(jnp.int32, (seqs, STATE_DIM), 0)
+    side = jnp.zeros((deep, LANES - STATE_DIM), F32)
+    gate = gate_ref[...].astype(F32)
+    gate = gate * sigmoid(gate)
+    direct = []
     for g in range(groups):
-        b_g = b_all[:, g * STATE_DIM:(g + 1) * STATE_DIM]
-        bt[g] = jnp.concatenate([b_g, b_g, b_g, b_pad], axis=0)
-    c_all = c_ref[...].astype(F32)
-    c_of = [c_all[:, g * STATE_DIM:(g + 1) * STATE_DIM].astype(BF16) for g in range(groups)]
-    k_rows = lax.broadcasted_iota(jnp.int32, (LANES, STATE_DIM), 0)
-    s_rows = lax.broadcasted_iota(jnp.int32, (seqs, span), 0)
-    acc[...] = jnp.zeros_like(acc)
-
-    def one_sequence(s, carry):
-        in_copy(s).wait()
-        row = dec[pl.ds(s, 1), :]
-        for g in range(groups):
-            picked = jnp.where(k_rows % seqs == s, bt[g], 0.0).astype(BF16)
-            outer = dot(lt[g * span:(g + 1) * span, :], picked)
-            fresh = []
-            for j in range(span // width):
-                h = g * (span // width) + j
-                rows = slice(h * width, (h + 1) * width)
-                new = state_v[s, rows, :] * row[:, h:h + 1] + outer[j * width:(j + 1) * width]
-                state_v[s, rows, :] = new
-                fresh.append(new.astype(BF16))
-            read = lax.dot_general(c_of[g], jnp.concatenate(fresh, axis=0), NT, preferred_element_type=F32)
-            columns = slice(g * span, (g + 1) * span)
-            acc[:, columns] = acc[:, columns] + jnp.where(s_rows == s, read, 0.0)
-        out_copy(s).start()
-        return carry
-
-    lax.fori_loop(0, seqs, one_sequence, 0)
-
-    gate = gate_ref[...].astype(F32)
-    gated = ((acc[...] + skip_wide * conv) * (gate * sigmoid(gate))).astype(BF16)
+        lanes = slice(g * STATE_DIM, (g + 1) * STATE_DIM)
+        columns = slice(g * span, (g + 1) * span)
+        b_g = b_all[:, lanes]
+        tall = jnp.concatenate([b_g, b_g, b_g, jnp.zeros((deep - 3 * seqs, STATE_DIM), F32)], axis=0)
+        tall = jnp.concatenate([tall, side], axis=1)
+        for s in range(seqs):
+            bt[g, :, s * LANES:(s + 1) * LANES] = jnp.where(b_rows % seqs == s, tall, 0.0).astype(BF16)
+        met = jnp.sum(b_g * c_all[:, lanes], axis=1, keepdims=True)
+        direct.append(fed[:, columns] * met + skip_wide[:, columns] * conv[:, columns])
+
     mixed = jnp.zeros((seqs, full), F32)
-    for k in range(CHUNKS):
-        w_copy(k).wait()
-        rows = slice(k * depth, (k + 1) * depth)
-        mixed = mixed + dot(gated[:, rows], wout_v[rows, :])
+    for g in range(groups):
+        columns = slice(g * span, (g + 1) * span)
+        c_g = c_all[:, g * STATE_DIM:(g + 1) * STATE_DIM]
+        in_copy(g).wait()
+        if g + 2 < groups:
+            in_copy(g + 2).start()
+            w_copy(g + 2).start()
+        read = jnp.zeros((seqs, span), F32)
+        for pair in range(seqs // 2):
+            outer = dot(lt[columns, :], bt[g, :, 2 * pair * LANES:2 * (pair + 1) * LANES])
+            for k in range(2):
+                s = 2 * pair + k
+                old = state_v[s, columns, :].astype(BF16)
+                picked = jnp.where(c_rows == s, c_g, 0.0).astype(BF16)
+                read = read + lax.dot_general(picked, old, NT, preferred_element_type=F32)
+                for j in range(span // width):
+                    h = g * (span // width) + j
+                    rows = slice(h * width, (h + 1) * width)
+                    state_v[s, rows, :] = (
+                        state_v[s, rows, :] * dec_b[h, s:s + 1, :]
+                        + outer[j * width:(j + 1) * width, k * LANES:k * LANES + STATE_DIM]
+                    )
+            out_copy(g, pair).start()
+        gated = ((decay_wide[:, columns] * read + direct[g]) * gate[:, columns]).astype(BF16)
+        w_copy(g).wait()
+        mixed = mixed + dot(gated, wout_v[columns, :])
+
     resid = (hidden_ref[...].astype(F32) + mixed.astype(BF16).astype(F32)).astype(BF16)
     resid_ref[...] = resid
     values = resid.astype(F32)
@@ -289,8 +308,9 @@
     for t, term in enumerate(three_terms(inv_rms)):
         extras = jnp.where(lane == 2 * FIELD + t, term, extras)
     packed_ref[:, full:] = extras.astype(BF16)
-    for s in range(seqs):
-        out_copy(s).wait()
+    for g in range(groups):
+        for pair in range(seqs // 2):
+            out_copy(g, pair).wait()
     for copy in hist_copies:
         copy.wait()
 
@@ -452,6 +472,7 @@
     line = n_ep // 4
     taps = convolution_history.shape[1]
     state = recurrent_state_matrix.reshape(seqs, inner, STATE_DIM)
+    deep = 4 * seqs
     dma = pltpu.SemaphoreType.DMA
     operands = (
         hidden, head_input_projected, output_gate_projected, input_map_projected,
@@ -471,14 +492,13 @@
         in_specs=[HBM_SPEC] * len(operands),
         out_specs=(VMEM_SPEC, VMEM_SPEC, HBM_SPEC, HBM_SPEC),
         scratch_shapes=[pltpu.VMEM(v.shape, v.dtype) for v in operands] + [
-            pltpu.VMEM((inner, LANES), BF16),
-            pltpu.VMEM((groups, LANES, STATE_DIM), F32),
-            pltpu.VMEM((seqs, heads), F32),
-            pltpu.VMEM((seqs, inner), F32),
+            pltpu.VMEM((inner, deep), BF16),
+            pltpu.VMEM((groups, deep, seqs * LANES), BF16),
+            pltpu.VMEM((heads, seqs, STATE_DIM), F32),
             dma((len(operands) - 2,)),
-            dma((seqs,)),
-            dma((CHUNKS,)),
-            dma((seqs,)),
+            dma((groups,)),
+            dma((groups,)),
+            dma((groups, seqs // 2)),
             dma((2,)),
         ],
         compiler_params=pltpu.CompilerParams(vmem_limit_bytes=MIXER_VMEM),

time: 38.9 us -> 36.7 us (0.943)
  Pallas kernels: 37.5 us -> 35.3 us
    pallas_call x1, Pallas kernels: 11.7 us -> 9.45 us  [on_device_kernels(): pl.pallas_call(mixer_kernel, out_shape=(pltpu.VMEM((seqs, full + LANES),...]
where the time goes in v1:
time: 36.7 us; the launch traced here: 36.6 us
  Pallas kernels  35.3 us (96%)
  between operations  0.65 us (2%)
  local copies, waits for them, and re-layouts  0.62 us (2%)
    pallas_call x1, Pallas kernels, on_device_kernels(): pl.pallas_call(functools.partial(expert_kernel, n_ep), out_shape=jax.Shap...  25.8 us
    pallas_call x1, Pallas kernels, on_device_kernels(): pl.pallas_call(mixer_kernel, out_shape=(pltpu.VMEM((seqs, full + LANES),...  9.45 us

profile of v1, /device:TPU:0, one launch (start us, length us, event | category | flops | bytes accessed | tf_op | source)
XLA Modules:
  0.0 36.6 jit_solution(7136662679133043166)
XLA Ops:
  0.6 9.5 %mixer.1 = (bf16[8,2176]{1,0:T(8,128)(2,1)S(1)}, bf16[8,2048]{1,0:T(8,128)(2,1)S(1)}, f32[8,2048,64]{2,1,0:T(8,128)}, bf16[3,8,2048]{2,1,0:T(8,128)(2,1)}) custom-call(bf16[8,2048]{1,0:T(8,128)(2,1)} %hidden_hbm.1, bf16[8,2048]{1,0:T(8,128)(2,1)} %head_in_hbm.1, bf16[8,2048]{1,0:T(8,128)(2,1)} %gate_hbm.1, bf16[8,256]{1,0:T(8,128)(2,1)} %b_hbm.1, ...), custom_call_target="tpu_custom_call" | custom-call | tf_op jit(solution)/shard_map/mixer/pallas_call | solution.py:484
  10.1 25.8 %experts.1 = bf16[8,2048]{1,0:T(8,128)(2,1)S(1)} custom-call(bf16[8,2176]{1,0:T(8,128)(2,1)S(1)} %get-tuple-element.7.packed_ref, bf16[8,2048]{1,0:T(8,128)(2,1)S(1)} %get-tuple-element.8.resid_ref, bf16[704,2048]{1,0:T(8,128)(2,1)} %bitcast.14, bf16[704,2048]{1,0:T(8,128)(2,1)} %bitcast.15, bf16[704,2048]{1,0:T(8,128)(2,1)} %bitcast.16), custom_call_target="tpu_custom_call" | custom-call | tf_op jit(solution)/shard_map/experts/pallas_call | solution.py:508
  35.9 0.6 %copy.23 = bf16[8,2048]{1,0:T(8,128)(2,1)} copy(bf16[8,2048]{1,0:T(8,128)(2,1)S(1)} %experts.1) | data formatting | bytes 65536
